TPU v7x, 32 devices: a whole 2x2x4 slice. The times are simulated.
32 devices in a mesh: sp: 16 (over z, y, x), dp: 2 (over core).
Axes of the slice: x: 2, y: 2, z: 4, core: 2. Of those that a mesh axis runs over, the one named last changes fastest.
Arguments:
- glu_value: bfloat16 [2, 8192, 512], P('dp', 'sp'), may hold values from -6 to 6
- glu_gate: bfloat16 [2, 8192, 512], P('dp', 'sp'), may hold values from -8 to 8
- cotangent: bfloat16 [2, 8192, 2048], P('dp', 'sp'), may hold values from -8 to 8
- conv_weight: float32 [31, 512], replicated, may hold values from -1 to 1
- norm_gain: float32 [512], replicated, may hold values from 0.1 to 1.9
- norm_shift: float32 [512], replicated, may hold values from -3 to 3
- out_weight: bfloat16 [2048, 512], P('dp'), may hold values from -0.25 to 0.25
Outputs:
- grad_value: bfloat16 [2, 8192, 512], P('dp', 'sp')
- grad_gate: bfloat16 [2, 8192, 512], P('dp', 'sp')
- grad_out_weight: float32 [2048, 512], P('dp')
- grad_conv: float32 [31, 512], replicated
- grad_gain: float32 [512], replicated
- grad_shift: float32 [512], replicated
All inputs are finite; a program needn't handle non-finite values.
Results may differ from a plain program's by a relative error of at most 0.003.
Values may be sent and summed in bfloat16 or wider, within the bound.
No kernel may reach another device: no remote copies, remote signals or barrier semaphores. Data moves between devices by JAX's collectives and lax.ppermute only.
A program may use at most 64 MiB of HBM per device.

v0:
```python
import math
import jax
import jax.numpy as jnp
from jax import lax
from jax.sharding import PartitionSpec as P

epsilon = 1e-06


def from_behind(value, axis, by):
    count = lax.axis_size(axis)
    pairs = [(i, i + by) for i in range(count) if 0 <= i + by < count]
    return lax.ppermute(value, axis, pairs)


def per_device(glu_value, glu_gate, cotangent, conv_weight, norm_gain, norm_shift, out_weight):
    value_rows = glu_value[0]
    gate_rows = glu_gate[0]
    cotan_rows = cotangent[0]
    length = value_rows.shape[0]
    channels = value_rows.shape[1]
    tap_count = conv_weight.shape[0]
    halo_rows = tap_count - 1
    count_sp = lax.axis_size("sp")
    count_dp = lax.axis_size("dp")
    scale = 1.0 / math.sqrt(length * count_sp * count_dp)
    prior_value, prior_gate = from_behind(
        (value_rows[length - halo_rows :], gate_rows[length - halo_rows :]), "sp", 1
    )
    value_ext = jnp.concatenate([prior_value, value_rows], axis=0).astype(jnp.float32)
    gate_ext = jnp.concatenate([prior_gate, gate_rows], axis=0).astype(jnp.float32)
    gated_ext = value_ext * jax.nn.sigmoid(gate_ext)
    conv_rows = jnp.zeros((length, channels), jnp.float32)
    for offset in range(tap_count):
        conv_rows = conv_rows + conv_weight[offset] * gated_ext[offset : offset + length]
    centred = conv_rows - jnp.mean(conv_rows, axis=-1, keepdims=True)
    inv_std = lax.rsqrt(jnp.mean(centred * centred, axis=-1, keepdims=True) + epsilon)
    normed = centred * inv_std
    pre_act = normed * norm_gain + norm_shift
    sigmoid_pre = jax.nn.sigmoid(pre_act)
    act_rows = (pre_act * sigmoid_pre).astype(jnp.bfloat16)
    columns = cotan_rows
    grad_act = jnp.dot(
        columns,
        lax.all_gather(out_weight, "dp", axis=0, tiled=True),
        preferred_element_type=jnp.float32,
    )
    grad_pre = grad_act * sigmoid_pre * (1.0 + pre_act * (1.0 - sigmoid_pre))
    grad_normed = grad_pre * norm_gain
    grad_conv_rows = inv_std * (
        grad_normed
        - jnp.mean(grad_normed, axis=-1, keepdims=True)
        - normed * jnp.mean(grad_normed * normed, axis=-1, keepdims=True)
    )
    later_grads = from_behind(grad_conv_rows[:halo_rows], "sp", -1)
    padded_grad = jnp.concatenate([grad_conv_rows, later_grads], axis=0)
    grad_gated = jnp.zeros((length, channels), jnp.float32)
    for offset in range(tap_count):
        start = tap_count - 1 - offset
        grad_gated = grad_gated + conv_weight[offset] * padded_grad[start : start + length]
    grad_taps = jnp.stack(
        [
            jnp.sum(grad_conv_rows * gated_ext[offset : offset + length], axis=0)
            for offset in range(tap_count)
        ],
        axis=0,
    )
    sigmoid_gate = jax.nn.sigmoid(gate_ext[halo_rows:])
    grad_value = (grad_gated * sigmoid_gate).astype(jnp.bfloat16)
    grad_gate = (grad_gated * value_ext[halo_rows:] * sigmoid_gate * (1.0 - sigmoid_gate)).astype(
        jnp.bfloat16
    )
    grad_conv, grad_gain, grad_shift = lax.psum(
        (
            grad_taps * scale,
            jnp.sum(grad_pre * normed, axis=0) * scale,
            jnp.sum(grad_pre, axis=0) * scale,
        ),
        ("sp", "dp"),
    )
    columns = cotan_rows
    product = lax.dot_general(
        columns, act_rows, (((0,), (0,)), ((), ())), preferred_element_type=jnp.float32
    )
    partial_rows = lax.psum_scatter(product * scale, "dp", scatter_dimension=0, tiled=True)
    grad_out_weight = lax.psum(partial_rows, "sp")
    return (grad_value[None], grad_gate[None], grad_out_weight, grad_conv, grad_gain, grad_shift)


def solution(mesh):
    in_specs = (
        P("dp", "sp", None),
        P("dp", "sp", None),
        P("dp", "sp", None),
        P(),
        P(),
        P(),
        P("dp", None),
    )
    out_specs = (P("dp", "sp", None), P("dp", "sp", None), P("dp", None), P(), P(), P())
    return jax.shard_map(
        per_device, mesh=mesh, in_specs=in_specs, out_specs=out_specs, check_vma=False
    )
```

profile of v0, /device:TPU:8, one launch (start us, length us, event | category | flops | bytes accessed | tf_op | source)
XLA Modules:
  0.0 316.3 jit_solution(10922288983692130966)
XLA Ops:
  7.2 0.0 copy-start
  7.2 0.0 copy-start.5
  7.2 0.0 all-gather.2.cloned.1.call-start
  7.2 0.7 all-gather.2.cloned.1.call-update
  7.9 0.0 reduce-scatter.2.cloned.1.call-start
  8.0 0.8 slice_bitcast_fusion
  8.7 3.4 %collective-permute-start.1 = (bf16[30,512]{1,0:T(8,128)(2,1)S(1)}, bf16[30,512]{1,0:T(8,128)(2,1)S(1)}, u32[]{:S(2)}, u32[]{:S(2)}) collective-permute-start(bf16[30,512]{1,0:T(8,128)(2,1)S(1)} %slice_bitcast_fusion), channel_id=1, source_target_pairs={{0,2},{2,4},{4,6},{6,8},{8,10},{10,12},{12,14},{14,16},{16,18},{18... | collective-permute-start | bytes 92168 | tf_op jit(solution)/shard_map/ppermute | solution.py:13
  12.2 0.8 slice_bitcast_fusion.1
  12.9 3.4 %collective-permute-start = (bf16[30,512]{1,0:T(8,128)(2,1)S(1)}, bf16[30,512]{1,0:T(8,128)(2,1)S(1)}, u32[]{:S(2)}, u32[]{:S(2)}) collective-permute-start(bf16[30,512]{1,0:T(8,128)(2,1)S(1)} %slice_bitcast_fusion.1), channel_id=1, source_target_pairs={{0,2},{2,4},{4,6},{6,8},{8,10},{10,12},{12,14},{14,16},{16,18},{18... | collective-permute-start | bytes 92168 | tf_op jit(solution)/shard_map/ppermute | solution.py:13
  16.3 0.0 copy-done.5
  16.4 0.0 collective-permute-done.1
  16.4 4.1 %collective-permute-done = bf16[30,512]{1,0:T(8,128)(2,1)S(1)} collective-permute-done((bf16[30,512]{1,0:T(8,128)(2,1)S(1)}, bf16[30,512]{1,0:T(8,128)(2,1)S(1)}, u32[]{:S(2)}, u32[]{:S(2)}) %collective-permute-start) | collective-permute-done | bytes 30752 | tf_op jit(solution)/shard_map/ppermute | solution.py:13
  20.5 1.6 divide_multiply_fusion
  22.1 0.0 copy-start.6
  22.2 0.0 copy-start.7
  22.2 5.0 %fusion.113 = (f32[512]{0:T(512)S(1)}, f32[512,512]{1,0:T(8,128)S(1)}) fusion(f32[542,512]{1,0:T(8,128)S(1)} %divide_multiply_fusion, f32[512]{0:T(512)S(1)} %bitcast.148, f32[512]{0:T(512)S(1)} %bitcast.150, f32[512]{0:T(512)S(1)} %bitcast.92, f32[512]{0:T(512)S(1)} %bitcast.94, f32[512]{0:T(512)S(1)} %bitcast.96, f32[512]{0:T(512)S(1)} %bitcast.98, ...), kind=kLoop, calls=%fused_computation.212 | loop fusion | flops 16252416 | bytes 33619968 | tf_op jit(solution)/shard_map/reduce_sum | solution.py:36
  27.2 0.0 copy-start.2
  27.2 0.3 multiply_reduce_fusion.33
  27.4 0.7 copy-done.2
  28.1 0.0 copy-done
  28.1 0.0 copy-done.6
  28.1 3.4 %multiply_bitcast_fusion = f32[2048,512]{0,1:T(8,128)} fusion(bf16[1,512,2048]{2,1,0:T(8,128)(2,1)S(1)} %copy-done, f32[512,512]{1,0:T(8,128)S(1)} %get-tuple-element.54, f32[512]{0:T(512)S(1)} %copy-done.7, f32[512]{0:T(512)S(1)} %copy-done.6, f32[512]{0:T(512)S(1)} %add_rsqrt_fusion, f32[512]{0:T(512)S(1)} %broadcast_multiply_fusion.5), kind=kOutput, calls=%fused_computation.29 | convolution fusion | flops 1077149696 | bytes 7348224 | tf_op jit(solution)/shard_map/dot_general | solution.py:82
  31.5 0.0 reduce-scatter.2.cloned.1.call-update
  31.5 0.0 all-reduce.4.cloned.1.call-start
  31.6 0.0 copy-start.4
  31.6 2.4 maximum_convert_fusion.1
  34.0 1.2 maximum_convert_fusion
  35.1 5.1 %multiply_reduce_fusion = (f32[512]{0:T(512)}, f32[512]{0:T(512)S(1)}, f32[512]{0:T(512)S(1)}, f32[512]{0:T(512)}, f32[512,512]{1,0:T(8,128)}) fusion(f32[512,512]{1,0:T(8,128)} %copy-done.2, f32[512]{0:T(512)S(1)} %add_rsqrt_fusion, f32[512]{0:T(512)S(1)} %broadcast_multiply_fusion.5, f32[512]{0:T(512)S(1)} %copy-done.6, f32[512]{0:T(512)S(1)} %copy-done.7, ...), kind=kOutput, calls=%fused_computation.151 | convolution fusion | flops 1078720512 | bytes 6307840 | tf_op jit(solution)/shard_map/dot_general | solution.py:43
  40.2 3.1 reduce-scatter.2.cloned.1.call-done
  43.3 0.0 all-reduce.4.cloned.1.call-update
  43.3 0.0 all-reduce.6.cloned.1.call-start
  43.4 4.2 %multiply_reduce_fusion.1 = (f32[512]{0:T(512)S(1)}, f32[512]{0:T(512)S(1)}, f32[512]{0:T(512)S(1)}, f32[512]{0:T(512)S(1)}, f32[512]{0:T(512)S(1)}, /*index=5*/...) fusion(f32[542,512]{1,0:T(8,128)S(1)} %divide_multiply_fusion, ...), kind=kLoop, calls=%fused_computation.152 | loop fusion | flops 11262976 | bytes 22067200 | tf_op jit(solution)/shard_map/reduce_sum | solution.py:63
  47.6 4.5 %collective-permute-start.2 = (f32[30,512]{1,0:T(8,128)S(1)}, f32[30,512]{1,0:T(8,128)S(1)}, u32[]{:S(2)}, u32[]{:S(2)}) collective-permute-start(f32[30,512]{1,0:T(8,128)S(1)} %slice.489), channel_id=1, source_target_pairs={{2,0},{4,2},{6,4},{8,6},{10,8},{12,10},{14,12},{16,14},{18,16},{20... | collective-permute-start | bytes 184328 | tf_op jit(solution)/shard_map/ppermute | solution.py:13
  52.0 2.3 multiply_reduce_fusion.19
  54.4 0.0 copy-done.1
  54.4 1.6 stack.127
  56.0 0.6 broadcast_multiply_fusion
  56.6 1.3 broadcast_multiply_fusion.1
  57.9 0.0 all-reduce.6.cloned.1.call-update
  57.9 0.0 collective-permute-done.2
  57.9 23.0 %fusion.105 = (bf16[1,512,512]{2,1,0:T(8,128)(2,1)}, f32[512,512]{1,0:T(8,128)S(1)}) fusion(f32[542,512]{1,0:T(8,128)} %maximum_convert_fusion, f32[542,512]{1,0:T(8,128)} %maximum_convert_fusion.1, f32[512,512]{1,0:T(8,128)} %copy-done.1, f32[512]{0:T(512)S(1)} %bitcast.149, f32[30,512]{1,0:T(8,128)S(1)} %collective-permute-done.2, f32[512]{0:T(512)S(1)} %bitcast.151, ...), kind=kLoop, calls=%fused_computation.196 | loop fusion | flops 25952256 | bytes 4843520 | tf_op jit(solution)/shard_map/broadcast_in_dim | solution.py:87
  81.0 1.1 fusion.104
  82.1 94.1 %all-reduce.4.cloned.1.call-done = f32[1024,512]{0,1:T(8,128)} async-done(((f32[1024,512]{0,1:T(8,128)}), f32[1024,512]{0,1:T(8,128)}) %all-reduce.4.cloned.1.call-update) | async-done | bytes 2097168 | tf_op jit(solution)/shard_map/psum | solution.py:86
  176.1 2.9 copy.13
  179.0 126.8 %all-reduce.6.cloned.1.call-done = (f32[31,512]{1,0:T(8,128)}, f32[512]{0:T(512)}, f32[512]{0:T(512)}) async-done(((f32[31,512]{1,0:T(8,128)}, f32[512]{0:T(512)}, f32[512]{0:T(512)}), (f32[31,512]{1,0:T(8,128)}, f32[512]{0:T(512)}, f32[512]{0:T(512)})) %all-reduce.6.cloned.1.call-update) | async-done | bytes 67600 | tf_op jit(solution)/shard_map/psum | solution.py:73
  305.8 1.5 copy.18
  307.3 1.3 copy.19
  308.6 1.2 copy.20
  (12 shorter events, 0.1 us)
Async XLA Ops:
  7.2 20.9 %copy-start = (bf16[1,512,2048]{2,1,0:T(8,128)(2,1)S(1)}, bf16[1,512,2048]{2,1,0:T(8,128)(2,1)}, u32[]{:S(2)}) copy-start(bf16[1,512,2048]{2,1,0:T(8,128)(2,1)} %param.9) | copy-start | bytes 6291460
  7.2 9.2 %copy-start.5 = (f32[31,512]{1,0:T(8,128)S(1)}, f32[31,512]{1,0:T(8,128)}, u32[]{:S(2)}) copy-start(f32[31,512]{1,0:T(8,128)} %param.10) | copy-start | bytes 190468
  7.2 27.9 %all-gather.2.cloned.1.call-start = ((), (), s32[]{:S(2)}) async-start(), calls=%async_computation.1 | async-start | bytes 3145728 | tf_op jit(solution)/shard_map/all_gather | solution.py:45
  7.9 35.4 %reduce-scatter.2.cloned.1.call-start = ((), (), s32[]{:S(2)}) async-start(), calls=%async_computation.2 | async-start | bytes 6291456 | tf_op jit(solution)/shard_map/reduce_scatter | solution.py:85
  8.7 7.7 %collective-permute-start.1 = (bf16[30,512]{1,0:T(8,128)(2,1)S(1)}, bf16[30,512]{1,0:T(8,128)(2,1)S(1)}, u32[]{:S(2)}, u32[]{:S(2)}) collective-permute-start(bf16[30,512]{1,0:T(8,128)(2,1)S(1)} %slice_bitcast_fusion), channel_id=1, source_target_pairs={{0,2},{2,4},{4,6},{6,8},{8,10},{10,12},{12,14},{14,16},{16,18},{18... | collective-permute-start | bytes 92168 | tf_op jit(solution)/shard_map/ppermute | solution.py:13
  12.9 7.6 %collective-permute-start = (bf16[30,512]{1,0:T(8,128)(2,1)S(1)}, bf16[30,512]{1,0:T(8,128)(2,1)S(1)}, u32[]{:S(2)}, u32[]{:S(2)}) collective-permute-start(bf16[30,512]{1,0:T(8,128)(2,1)S(1)} %slice_bitcast_fusion.1), channel_id=1, source_target_pairs={{0,2},{2,4},{4,6},{6,8},{8,10},{10,12},{12,14},{14,16},{16,18},{18... | collective-permute-start | bytes 92168 | tf_op jit(solution)/shard_map/ppermute | solution.py:13
  22.1 6.0 %copy-start.6 = (f32[512]{0:T(512)S(1)}, f32[512]{0:T(512)}, u32[]{:S(2)}) copy-start(f32[512]{0:T(512)} %param.11) | copy-start | bytes 6148
  22.2 6.0 %copy-start.7 = (f32[512]{0:T(512)S(1)}, f32[512]{0:T(512)}, u32[]{:S(2)}) copy-start(f32[512]{0:T(512)} %param.12) | copy-start | bytes 6148
  27.2 1.0 copy-start.2
  31.5 144.6 %all-reduce.4.cloned.1.call-start = ((), (), s32[]{:S(2)}) async-start(), calls=%async_computation.3 | async-start | bytes 4194304 | tf_op jit(solution)/shard_map/psum | solution.py:86
  31.6 2.4 copy-start.4
  43.3 262.5 %all-reduce.6.cloned.1.call-start = ((), (), s32[]{:S(2)}) async-start(), calls=%async_computation.4 | async-start | bytes 139264 | tf_op jit(solution)/shard_map/psum | solution.py:73
  47.6 6.8 %copy-start.1 = (f32[512,512]{1,0:T(8,128)}, f32[512,512]{1,0:T(8,128)S(1)}, u32[]{:S(2)}) copy-start(f32[512,512]{1,0:T(8,128)S(1)} %get-tuple-element.50) | copy-start | bytes 3145732
  47.6 10.3 %collective-permute-start.2 = (f32[30,512]{1,0:T(8,128)S(1)}, f32[30,512]{1,0:T(8,128)S(1)}, u32[]{:S(2)}, u32[]{:S(2)}) collective-permute-start(f32[30,512]{1,0:T(8,128)S(1)} %slice.489), channel_id=1, source_target_pairs={{2,0},{4,2},{6,4},{8,6},{10,8},{12,10},{14,12},{16,14},{18,16},{20... | collective-permute-start | bytes 184328 | tf_op jit(solution)/shard_map/ppermute | solution.py:13
  57.9 23.1 %copy-start.3 = (f32[542,512]{1,0:T(8,128)S(1)}, f32[542,512]{1,0:T(8,128)}, u32[]{:S(2)}) copy-start(f32[542,512]{1,0:T(8,128)} %maximum_convert_fusion.1) | copy-start | bytes 3330052
Sparse Core Ops, SparseCore 0:
  9.5 11.9 all-gather.1
  31.7 11.5 reduce-scatter.1
  48.8 127.2 all-reduce.3
  182.5 123.2 all-reduce.5
where the time goes:
time: 317 us; the launch traced here: 316 us
  waiting for transfers between devices  229 us (72%)
  other arithmetic  42.9 us (14%)
  between operations  14 us (4%)
  starting transfers between devices  11.4 us (4%)
  local copies, waits for them, and re-layouts  10.7 us (3%)
  matrix products  8.5 us (3%)
    psum x1, waiting for transfers between devices, per_device(): lax.psum((grad_taps * scale, jnp.sum(grad_pre * normed, axis=0) * scale,...  127 us
    psum x1, waiting for transfers between devices, per_device(): grad_out_weight = lax.psum(partial_rows, 'sp')  94.1 us
    broadcast_in_dim x1, other arithmetic, per_device(): grad_gate[None]  23 us
    ppermute x3, starting transfers between devices, from_behind(): return lax.ppermute(value, axis, pairs)  11.2 us
    unnamed x20, local copies, waits for them, and re-layouts  7.56 us
    reduce_sum x2, other arithmetic, per_device(): jnp.sum(grad_conv_rows * gated_ext[offset:offset + length], axis=0)  6.52 us
  transfers between devices with their start and end apart: 7, of which 4 were waited for; matrix products, arithmetic and copies ran while one was open for 18% of the time, Pallas kernels for 0%

commit v1 on v0

--- a/solution.py
+++ b/solution.py
@@ -83,7 +83,14 @@
         columns, act_rows, (((0,), (0,)), ((), ())), preferred_element_type=jnp.float32
     )
     partial_rows = lax.psum_scatter(product * scale, "dp", scatter_dimension=0, tiled=True)
-    grad_out_weight = lax.psum(partial_rows, "sp")
+    n_all = jax.lax.axis_size("sp")
+    grad_out_weight, f_next = (partial_rows, 0)
+    while 1 << f_next < n_all:
+        k_now = jax.lax.ppermute(
+            grad_out_weight, "sp", perm=[(no, no ^ 1 << f_next) for no in range(n_all)]
+        )
+        grad_out_weight = grad_out_weight + k_now
+        f_next = f_next + 1
     return (grad_value[None], grad_gate[None], grad_out_weight, grad_conv, grad_gain, grad_shift)
 
 

time: 317 us -> 396 us (1.25)
  waiting for transfers between devices: 229 us -> 302 us
  starting transfers between devices: 11.4 us -> 18.2 us
    ppermute x0 -> x4, waiting for transfers between devices: none -> 196 us  [per_device(): jax.lax.ppermute(grad_out_weight, 'sp', perm=[(no, no ^ 1 << f_next) for...]
    psum x1 -> x0, waiting for transfers between devices: 94.1 us -> none  [per_device(): grad_out_weight = lax.psum(partial_rows, 'sp')]
    psum x1, waiting for transfers between devices: 127 us -> 91.5 us  [per_device(): lax.psum((grad_taps * scale, jnp.sum(grad_pre * normed, axis=0) * scale,...]
    broadcast_in_dim x1, other arithmetic: 23 us -> 7.23 us  [per_device(): grad_gate[None]]
    add x0 -> x4, other arithmetic: none -> 15.6 us  [per_device(): grad_out_weight = grad_out_weight + k_now]
    reduce_scatter x1, waiting for transfers between devices: 3.07 us -> 11.7 us  [per_device(): lax.psum_scatter(product * scale, 'dp', scatter_dimension=0, tiled=True)]
    ppermute x0 -> x4, starting transfers between devices: none -> 5.81 us  [per_device(): jax.lax.ppermute(grad_out_weight, 'sp', perm=[(no, no ^ 1 << f_next) for...]
  transfers between devices with their start and end apart: 7 -> 10, of which waited for: 4 -> 7; matrix products, arithmetic and copies ran while one was open for 18% -> 11% of each run, Pallas kernels for 0% -> 0%
where the time goes in v1:
time: 396 us; the launch traced here: 395 us
  waiting for transfers between devices  302 us (76%)
  other arithmetic  40.9 us (10%)
  starting transfers between devices  18.2 us (5%)
  between operations  13.9 us (4%)
  local copies, waits for them, and re-layouts  13 us (3%)
  matrix products  7.72 us (2%)
    ppermute x4, waiting for transfers between devices, per_device(): jax.lax.ppermute(grad_out_weight, 'sp', perm=[(no, no ^ 1 << f_next) for...  196 us
    psum x1, waiting for transfers between devices, per_device(): lax.psum((grad_taps * scale, jnp.sum(grad_pre * normed, axis=0) * scale,...  91.5 us
    add x4, other arithmetic, per_device(): grad_out_weight = grad_out_weight + k_now  15.6 us
    ppermute x3, starting transfers between devices, from_behind(): return lax.ppermute(value, axis, pairs)  12.2 us
    reduce_scatter x1, waiting for transfers between devices, per_device(): lax.psum_scatter(product * scale, 'dp', scatter_dimension=0, tiled=True)  11.7 us
  transfers between devices with their start and end apart: 10, of which 7 were waited for; matrix products, arithmetic and copies ran while one was open for 11% of the time, Pallas kernels for 0%

profile of v1, /device:TPU:8, one launch (start us, length us, event | category | flops | bytes accessed | tf_op | source)
XLA Modules:
  0.0 395.5 jit_solution(1175594970375216227)
XLA Ops:
  7.2 0.0 copy-start
  7.2 0.0 reduce-scatter.2.cloned.1.call-start
  7.2 0.9 slice_bitcast_fusion
  8.1 3.4 collective-permute-start.1
  11.5 0.8 slice_bitcast_fusion.1
  12.3 3.4 collective-permute-start
  15.7 1.1 fusion.114
  16.9 1.0 fusion.115
  17.9 2.0 collective-permute-done
  19.9 1.6 divide_multiply_fusion
  21.6 5.0 %fusion.113 = (f32[512]{0:T(512)S(1)}, f32[512,512]{1,0:T(8,128)S(1)}) fusion(f32[542,512]{1,0:T(8,128)S(1)} %divide_multiply_fusion, f32[512]{0:T(512)S(1)} %bitcast.148, f32[512]{0:T(512)S(1)} %bitcast.150, f32[512]{0:T(512)S(1)} %bitcast.92, f32[512]{0:T(512)S(1)} %bitcast.94, f32[512]{0:T(512)S(1)} %bitcast.96, f32[512]{0:T(512)S(1)} %bitcast.98, ...), kind=kLoop, calls=%fused_computation.212 | loop fusion | flops 16252416 | bytes 33619968 | tf_op jit(solution)/shard_map/reduce_sum | solution.py:36
  26.6 0.3 multiply_reduce_fusion.33
  26.8 0.7 copy-done.3
  27.6 3.4 multiply_bitcast_fusion
  30.9 0.0 reduce-scatter.2.cloned.1.call-update
  31.0 0.0 all-gather.2.cloned.1.call-start
  31.0 11.7 %reduce-scatter.2.cloned.1.call-done = f32[1024,512]{0,1:T(8,128)} async-done(((f32[2048,512]{0,1:T(8,128)}), f32[1024,512]{0,1:T(8,128)}) %reduce-scatter.2.cloned.1.call-update) | async-done | bytes 2097168 | tf_op jit(solution)/shard_map/reduce_scatter | solution.py:85
  42.7 1.5 collective-permute-start.3
  44.2 46.5 %collective-permute-done.3 = f32[1024,512]{0,1:T(8,128)S(1)} collective-permute-done((f32[1024,512]{0,1:T(8,128)}, f32[1024,512]{0,1:T(8,128)S(1)}, u32[]{:S(2)}, u32[]{:S(2)}) %collective-permute-start.3) | collective-permute-done | bytes 2097184 | tf_op jit(solution)/shard_map/ppermute | solution.py:89
  90.6 3.3 add.299
  93.9 1.5 collective-permute-start.4
  95.4 0.0 all-gather.2.cloned.1.call-update
  95.4 0.0 all-reduce.3.cloned.1.call-start
  95.5 2.3 maximum_convert_fusion.1
  97.8 1.2 maximum_convert_fusion
  98.9 42.2 %collective-permute-done.4 = f32[1024,512]{0,1:T(8,128)} collective-permute-done((f32[1024,512]{0,1:T(8,128)}, f32[1024,512]{0,1:T(8,128)}, u32[]{:S(2)}, u32[]{:S(2)}) %collective-permute-start.4) | collective-permute-done | bytes 2097184 | tf_op jit(solution)/shard_map/ppermute | solution.py:89
  141.1 4.1 %add.300 = f32[1024,512]{0,1:T(8,128)} add(f32[1024,512]{0,1:T(8,128)} %add.299, f32[1024,512]{0,1:T(8,128)} %collective-permute-done.4) | non-fusion elementwise | flops 524288 | bytes 6291456 | tf_op jit(solution)/shard_map/add | solution.py:92
  145.2 0.5 collective-permute-start.5
  145.7 4.3 %multiply_reduce_fusion = (f32[512]{0:T(512)}, f32[512]{0:T(512)S(1)}, f32[512]{0:T(512)S(1)}, f32[512]{0:T(512)}, f32[512,512]{1,0:T(8,128)S(1)}) fusion(f32[512,512]{1,0:T(8,128)} %copy-done.3, f32[512]{0:T(512)S(1)} %add_rsqrt_fusion, f32[512]{0:T(512)S(1)} %broadcast_multiply_fusion.5, f32[512]{0:T(512)S(1)} %copy-done.7, f32[512]{0:T(512)S(1)} %copy-done.10, ...), kind=kOutput, calls=%fused_computation.151 | convolution fusion | flops 1078720512 | bytes 6307840 | tf_op jit(solution)/shard_map/dot_general | solution.py:43
  150.0 3.2 multiply_reduce_fusion.1
  153.2 5.4 %collective-permute-start.2 = (f32[30,512]{1,0:T(8,128)S(1)}, f32[30,512]{1,0:T(8,128)S(1)}, u32[]{:S(2)}, u32[]{:S(2)}) collective-permute-start(f32[30,512]{1,0:T(8,128)S(1)} %slice.489), channel_id=1, source_target_pairs={{2,0},{4,2},{6,4},{8,6},{10,8},{12,10},{14,12},{16,14},{18,16},{20... | collective-permute-start | bytes 184328 | tf_op jit(solution)/shard_map/ppermute | solution.py:13
  158.7 2.3 multiply_reduce_fusion.19
  161.0 1.6 stack.127
  162.6 28.9 %collective-permute-done.5 = f32[1024,512]{0,1:T(8,128)} collective-permute-done((f32[1024,512]{0,1:T(8,128)}, f32[1024,512]{0,1:T(8,128)}, u32[]{:S(2)}, u32[]{:S(2)}) %collective-permute-start.5) | collective-permute-done | bytes 2097184 | tf_op jit(solution)/shard_map/ppermute | solution.py:89
  191.5 4.1 %add.301 = f32[1024,512]{0,1:T(8,128)} add(f32[1024,512]{0,1:T(8,128)} %add.300, f32[1024,512]{0,1:T(8,128)} %collective-permute-done.5) | non-fusion elementwise | flops 524288 | bytes 6291456 | tf_op jit(solution)/shard_map/add | solution.py:92
  195.6 2.4 collective-permute-start.6
  198.0 0.6 broadcast_multiply_fusion
  198.7 0.6 broadcast_multiply_fusion.1
  199.3 0.0 all-reduce.3.cloned.1.call-update
  199.3 7.2 %fusion.105 = (bf16[1,512,512]{2,1,0:T(8,128)(2,1)}, f32[512,512]{1,0:T(8,128)S(1)}) fusion(f32[542,512]{1,0:T(8,128)} %maximum_convert_fusion, f32[542,512]{1,0:T(8,128)} %maximum_convert_fusion.1, f32[512,512]{1,0:T(8,128)S(1)} %copy-done.2, f32[512]{0:T(512)S(1)} %bitcast.149, f32[30,512]{1,0:T(8,128)S(1)} %collective-permute-done.2, ...), kind=kLoop, calls=%fused_computation.196 | loop fusion | flops 25952256 | bytes 4843520 | tf_op jit(solution)/shard_map/broadcast_in_dim | solution.py:94
  206.5 1.1 fusion.104
  207.6 78.9 %collective-permute-done.6 = f32[1024,512]{0,1:T(8,128)} collective-permute-done((f32[1024,512]{0,1:T(8,128)}, f32[1024,512]{0,1:T(8,128)}, u32[]{:S(2)}, u32[]{:S(2)}) %collective-permute-start.6) | collective-permute-done | bytes 2097184 | tf_op jit(solution)/shard_map/ppermute | solution.py:89
  286.5 4.1 %add.302 = f32[1024,512]{0,1:T(8,128)} add(f32[1024,512]{0,1:T(8,128)} %add.301, f32[1024,512]{0,1:T(8,128)} %collective-permute-done.6) | non-fusion elementwise | flops 524288 | bytes 6291456 | tf_op jit(solution)/shard_map/add | solution.py:92
  290.6 2.9 copy.13
  293.4 91.5 %all-reduce.3.cloned.1.call-done = (f32[31,512]{1,0:T(8,128)}, f32[512]{0:T(512)}, f32[512]{0:T(512)}) async-done(((f32[31,512]{1,0:T(8,128)}, f32[512]{0:T(512)}, f32[512]{0:T(512)}), (f32[31,512]{1,0:T(8,128)}, f32[512]{0:T(512)}, f32[512]{0:T(512)})) %all-reduce.3.cloned.1.call-update) | async-done | bytes 67600 | tf_op jit(solution)/shard_map/psum | solution.py:73
  385.0 1.5 copy.17
  386.5 1.2 copy.18
  387.7 1.2 copy.19
  (27 shorter events, 0.1 us)
Async XLA Ops:
  7.2 20.4 %copy-start = (bf16[1,512,2048]{2,1,0:T(8,128)(2,1)S(1)}, bf16[1,512,2048]{2,1,0:T(8,128)(2,1)}, u32[]{:S(2)}) copy-start(bf16[1,512,2048]{2,1,0:T(8,128)(2,1)} %param.9) | copy-start | bytes 6291460
  7.2 35.5 %reduce-scatter.2.cloned.1.call-start = ((), (), s32[]{:S(2)}) async-start(), calls=%async_computation.2 | async-start | bytes 6291456 | tf_op jit(solution)/shard_map/reduce_scatter | solution.py:85
  8.1 9.8 %collective-permute-start.1 = (bf16[30,512]{1,0:T(8,128)(2,1)S(1)}, bf16[30,512]{1,0:T(8,128)(2,1)S(1)}, u32[]{:S(2)}, u32[]{:S(2)}) collective-permute-start(bf16[30,512]{1,0:T(8,128)(2,1)S(1)} %slice_bitcast_fusion), channel_id=1, source_target_pairs={{0,2},{2,4},{4,6},{6,8},{8,10},{10,12},{12,14},{14,16},{16,18},{18... | collective-permute-start | bytes 92168 | tf_op jit(solution)/shard_map/ppermute | solution.py:13
  12.3 7.6 %collective-permute-start = (bf16[30,512]{1,0:T(8,128)(2,1)S(1)}, bf16[30,512]{1,0:T(8,128)(2,1)S(1)}, u32[]{:S(2)}, u32[]{:S(2)}) collective-permute-start(bf16[30,512]{1,0:T(8,128)(2,1)S(1)} %slice_bitcast_fusion.1), channel_id=1, source_target_pairs={{0,2},{2,4},{4,6},{6,8},{8,10},{10,12},{12,14},{14,16},{16,18},{18... | collective-permute-start | bytes 92168 | tf_op jit(solution)/shard_map/ppermute | solution.py:13
  21.5 6.0 %copy-start.7 = (f32[512]{0:T(512)S(1)}, f32[512]{0:T(512)}, u32[]{:S(2)}) copy-start(f32[512]{0:T(512)} %param.11) | copy-start | bytes 6148
  21.5 6.0 %copy-start.10 = (f32[512]{0:T(512)S(1)}, f32[512]{0:T(512)}, u32[]{:S(2)}) copy-start(f32[512]{0:T(512)} %param.12) | copy-start | bytes 6148
  26.5 1.0 copy-start.3
  31.0 114.7 %all-gather.2.cloned.1.call-start = ((), (), s32[]{:S(2)}) async-start(), calls=%async_computation.1 | async-start | bytes 3145728 | tf_op jit(solution)/shard_map/all_gather | solution.py:45
  42.7 47.9 %collective-permute-start.3 = (f32[1024,512]{0,1:T(8,128)}, f32[1024,512]{0,1:T(8,128)S(1)}, u32[]{:S(2)}, u32[]{:S(2)}) collective-permute-start(f32[1024,512]{0,1:T(8,128)} %reduce-scatter.2.cloned.1.call-done), channel_id=1, source_target_pairs={{0,2},{2,0},{4,6},{6,4},{8,10},{10,8},{12,14},{14,12},{16,18},{18,... | collective-permute-start | bytes 6291464 | tf_op jit(solution)/shard_map/ppermute | solution.py:89
  93.9 47.2 %collective-permute-start.4 = (f32[1024,512]{0,1:T(8,128)}, f32[1024,512]{0,1:T(8,128)}, u32[]{:S(2)}, u32[]{:S(2)}) collective-permute-start(f32[1024,512]{0,1:T(8,128)} %add.299), channel_id=1, source_target_pairs={{0,4},{2,6},{4,0},{6,2},{8,12},{10,14},{12,8},{14,10},{16,20},{18,... | collective-permute-start | bytes 6291464 | tf_op jit(solution)/shard_map/ppermute | solution.py:89
  95.4 289.5 %all-reduce.3.cloned.1.call-start = ((), (), s32[]{:S(2)}) async-start(), calls=%async_computation.3 | async-start | bytes 139264 | tf_op jit(solution)/shard_map/psum | solution.py:73
  95.5 2.3 copy-start.6
  145.2 46.3 %collective-permute-start.5 = (f32[1024,512]{0,1:T(8,128)}, f32[1024,512]{0,1:T(8,128)}, u32[]{:S(2)}, u32[]{:S(2)}) collective-permute-start(f32[1024,512]{0,1:T(8,128)} %add.300), channel_id=1, source_target_pairs={{0,8},{2,10},{4,12},{6,14},{8,0},{10,2},{12,4},{14,6},{16,24},{18,... | collective-permute-start | bytes 6291464 | tf_op jit(solution)/shard_map/ppermute | solution.py:89
  145.7 4.3 %copy-start.4 = (f32[512,512]{1,0:T(8,128)S(1)}, f32[512,512]{1,0:T(8,128)}, u32[]{:S(2)}) copy-start(f32[512,512]{1,0:T(8,128)} %copy-done.3) | copy-start | bytes 3145732
  153.2 7.8 %copy-start.1 = (f32[512,512]{1,0:T(8,128)}, f32[512,512]{1,0:T(8,128)S(1)}, u32[]{:S(2)}) copy-start(f32[512,512]{1,0:T(8,128)S(1)} %get-tuple-element.50) | copy-start | bytes 3145732
  153.2 46.1 %collective-permute-start.2 = (f32[30,512]{1,0:T(8,128)S(1)}, f32[30,512]{1,0:T(8,128)S(1)}, u32[]{:S(2)}, u32[]{:S(2)}) collective-permute-start(f32[30,512]{1,0:T(8,128)S(1)} %slice.489), channel_id=1, source_target_pairs={{2,0},{4,2},{6,4},{8,6},{10,8},{12,10},{14,12},{16,14},{18,16},{20... | collective-permute-start | bytes 184328 | tf_op jit(solution)/shard_map/ppermute | solution.py:13
  162.6 36.1 %copy-start.8 = (f32[512]{0:T(512)S(1)}, f32[512]{0:T(512)}, u32[]{:S(2)}) copy-start(f32[512]{0:T(512)} %get-tuple-element.43) | copy-start | bytes 6148
  162.6 36.1 %copy-start.9 = (f32[512]{0:T(512)S(1)}, f32[512]{0:T(512)}, u32[]{:S(2)}) copy-start(f32[512]{0:T(512)} %get-tuple-element.46) | copy-start | bytes 6148
  162.6 36.7 %copy-start.2 = (f32[512,512]{1,0:T(8,128)S(1)}, f32[512,512]{1,0:T(8,128)}, u32[]{:S(2)}) copy-start(f32[512,512]{1,0:T(8,128)} %copy-done.1) | copy-start | bytes 3145732
  195.6 90.9 %collective-permute-start.6 = (f32[1024,512]{0,1:T(8,128)}, f32[1024,512]{0,1:T(8,128)}, u32[]{:S(2)}, u32[]{:S(2)}) collective-permute-start(f32[1024,512]{0,1:T(8,128)} %add.301), channel_id=1, source_target_pairs={{0,16},{2,18},{4,20},{6,22},{8,24},{10,26},{12,28},{14,30},{16,0},... | collective-permute-start | bytes 6291464 | tf_op jit(solution)/shard_map/ppermute | solution.py:89
  199.3 7.3 %copy-start.5 = (f32[542,512]{1,0:T(8,128)S(1)}, f32[542,512]{1,0:T(8,128)}, u32[]{:S(2)}) copy-start(f32[542,512]{1,0:T(8,128)} %maximum_convert_fusion.1) | copy-start | bytes 3330052
Sparse Core Ops, SparseCore 0:
  31.1 11.5 reduce-scatter.1
  95.5 10.8 all-gather.1
  199.4 185.5 all-reduce.2
